TPU v7x, 32 devices: a whole 2x2x4 slice. The times are simulated.
32 devices in a mesh: sp: 16 (over z, y, core), tp: 2 (over x).
Axes of the slice: x: 2, y: 2, z: 4, core: 2. Of those that a mesh axis runs over, the one named last changes fastest.
Arguments:
- query_latent: bfloat16 [4096, 1024], P('sp'), may hold values from -6 to 6
- shared_latent: bfloat16 [4096, 512], P('sp'), may hold values from -25 to 25
- rotary_key: bfloat16 [4096, 64], P('sp'), may hold values from -300 to 300
- document_start: int32 [4096], P('sp'), may hold values from 0 to 4095, as said below
- query_gain: float32 [1024], replicated, may hold values from 0.1 to 1.9
- shared_gain: float32 [512], replicated, may hold values from 0.1 to 1.9
- content_weight: bfloat16 [1024, 2048], P(None, 'tp'), may hold values from -0.1875 to 0.1875
- rotary_weight: bfloat16 [1024, 1024], P(None, 'tp'), may hold values from -0.1875 to 0.1875
- key_weight: bfloat16 [512, 2048], P(None, 'tp'), may hold values from -0.25 to 0.25
- value_weight: bfloat16 [512, 2048], P(None, 'tp'), may hold values from -0.25 to 0.25
- output_weight: bfloat16 [2048, 4096], P('tp'), may hold values from -0.125 to 0.125
Outputs:
- mixed: bfloat16 [4096, 4096], P('sp')
Inputs may be any that keep to these rules, and one draw needn't show every extreme that they name: `document_start`: each position holds the first position of its document; documents are runs of 1 to 1792 consecutive positions and one of them has exactly 1792; the values never fall.
All inputs are finite; a program needn't handle non-finite values.
Results may differ from a plain program's by a relative error of at most 0.038.
The roundings to bfloat16 on the way count: a program that leaves them out, or rounds other values in their place, can miss the bound.
Values may be sent and summed in bfloat16 or wider, within the bound.
A program may use at most 64 MiB of HBM per device.

v0:
```python
import jax
import jax.numpy as jnp
from jax import lax
from jax.sharding import PartitionSpec as P

MODEL = 4096
CONTENT = 128
ROTARY = 64
VALUE_DIM = 128
SPAN = 8


norm_eps = 1e-06
rope_theta = 10000.0
masked_score = -1e30


def from_behind(value, axis, steps):
    count = lax.axis_size(axis)
    initial, last = (max(0, -steps), min(count, count - steps))
    return lax.ppermute(value, axis, [(source, source + steps) for source in range(initial, last)])


def rms_scale(latent, scaling):
    entries = latent.astype(jnp.float32)
    scaled = entries * lax.rsqrt(jnp.mean(entries * entries, axis=-1, keepdims=True) + norm_eps)
    return (scaled * scaling).astype(jnp.bfloat16)


def rotate(entries, places):
    width = entries.shape[-1]
    halfway = width // 2
    frequency = 1.0 / rope_theta ** (jnp.arange(0, width, 2, dtype=jnp.float32) / width)
    angles = places.astype(jnp.float32)[:, None] * frequency[None, :]
    target = (angles.shape[0],) + (1,) * (entries.ndim - 2) + (halfway,)
    cosine_table = jnp.cos(angles).reshape(target)
    sine_table = jnp.sin(angles).reshape(target)
    leading = entries[..., :halfway]
    trailing = entries[..., halfway:]
    return jnp.concatenate(
        [
            leading * cosine_table - trailing * sine_table,
            leading * sine_table + trailing * cosine_table,
        ],
        axis=-1,
    )


def expand(shared_block, key_weight, value_weight):
    expanded_keys = jnp.dot(shared_block, key_weight, preferred_element_type=jnp.float32).astype(
        jnp.bfloat16
    )
    expanded_values = jnp.dot(
        shared_block, value_weight, preferred_element_type=jnp.float32
    ).astype(jnp.bfloat16)
    return (expanded_keys, expanded_values)


def on_device(
    query_latent,
    shared_latent,
    rotary_key,
    document_start,
    query_gain,
    shared_gain,
    content_weight,
    rotary_weight,
    key_weight,
    value_weight,
    output_weight,
):
    length = query_latent.shape[0]
    anchor = lax.axis_index("sp") * length
    head_count = key_weight.shape[1] // CONTENT
    places = anchor + jnp.arange(length, dtype=jnp.int32)
    query_rows = rms_scale(query_latent, query_gain)
    shared_rows = rms_scale(shared_latent, shared_gain)
    turn_rows = rotate(rotary_key.astype(jnp.float32), places).astype(jnp.bfloat16)
    query_content = (
        jnp.dot(query_rows, content_weight, preferred_element_type=jnp.float32)
        .astype(jnp.bfloat16)
        .reshape(length, head_count, CONTENT)
    )
    query_raw = jnp.dot(query_rows, rotary_weight, preferred_element_type=jnp.float32).reshape(
        length, head_count, ROTARY
    )
    query_turn = rotate(query_raw, places).astype(jnp.bfloat16)
    first_start = document_start[0]
    score_scale = (CONTENT + ROTARY) ** (-0.5)
    payload = (shared_rows, turn_rows)

    def absorb(softmax_state, arrived, distance):
        block_anchor = anchor - distance * length

        def update(current):
            block_shared, block_turn = arrived
            block_keys, block_values = expand(block_shared, key_weight, value_weight)
            block_keys = block_keys.reshape(length, head_count, CONTENT)
            block_values = block_values.reshape(length, head_count, VALUE_DIM)
            scores = jnp.einsum(
                "qhd,khd->hqk", query_content, block_keys, preferred_element_type=jnp.float32
            )
            scores = scores + jnp.einsum(
                "qhr,kr->hqk", query_turn, block_turn, preferred_element_type=jnp.float32
            )
            key_places = block_anchor + jnp.arange(length, dtype=jnp.int32)
            visible = (key_places[None, :] >= document_start[:, None]) & (
                key_places[None, :] <= places[:, None]
            )
            scores = jnp.where(visible[None], scores * score_scale, masked_score)
            running, denominator, summed = current
            highest = jnp.maximum(running, jnp.max(scores, axis=-1))
            factor = jnp.exp(running - highest)
            weights = jnp.exp(scores - highest[:, :, None])
            denominator = denominator * factor + jnp.sum(weights, axis=-1)
            summed = summed * factor[:, :, None] + jnp.einsum(
                "hqk,khd->hqd",
                weights.astype(jnp.bfloat16),
                block_values,
                preferred_element_type=jnp.float32,
            )
            return (highest, denominator, summed)

        def unchanged(current):
            return current

        needed = (block_anchor >= 0) & (block_anchor + length - 1 >= first_start)
        return lax.cond(needed, update, unchanged, softmax_state)

    initial = (
        jnp.full((head_count, length), masked_score, jnp.float32),
        jnp.zeros((head_count, length), jnp.float32),
        jnp.zeros((head_count, length, VALUE_DIM), jnp.float32),
    )
    softmax_state = absorb(initial, payload, 0)

    def advance(counter, carried):
        moving, current = carried
        moving = from_behind((moving[0], moving[1]), "sp", 1)
        return (moving, absorb(current, moving, counter + 1))

    moving, softmax_state = lax.fori_loop(0, SPAN - 1, advance, (payload, softmax_state))
    highest, denominator, summed = softmax_state
    attended = (summed / denominator[:, :, None]).astype(jnp.bfloat16)
    weight_heads = output_weight.reshape(head_count, VALUE_DIM, MODEL)
    group_term = jnp.einsum(
        "hqd,hdm->qm", attended, weight_heads, preferred_element_type=jnp.float32
    ).astype(jnp.bfloat16)
    group_term = lax.optimization_barrier(group_term).astype(jnp.float32)
    mixed = lax.psum(group_term.astype(jnp.bfloat16), "tp")
    return mixed


def solution(mesh):
    return jax.shard_map(
        on_device,
        mesh=mesh,
        in_specs=(
            P("sp", None),
            P("sp", None),
            P("sp", None),
            P("sp"),
            P(),
            P(),
            P(None, "tp"),
            P(None, "tp"),
            P(None, "tp"),
            P(None, "tp"),
            P("tp", None),
        ),
        out_specs=P("sp", None),
        check_vma=False,
    )
```

profile of v0, /device:TPU:16, one launch (start us, length us, event | category | flops | bytes accessed | tf_op | source)
XLA Modules:
  0.0 222.1 jit_solution(5317073133441367061)
XLA Ops:
  6.6 0.9 convert_element_type.72
  7.5 1.2 fusion.33
  8.7 2.8 %fusion.40 = f32[256,512]{0,1:T(8,128)} fusion(bf16[1024,512]{1,0:T(8,128)(2,1)} %param.24, bf16[256,1024]{1,0:T(8,128)(2,1)} %param.17, f32[1024]{0:T(1024)} %param.21, f32[256]{0:T(256)S(1)} %add_rsqrt_fusion), kind=kOutput, calls=%fused_computation.67 | convolution fusion | flops 269484032 | bytes 2102272 | tf_op jit(solution)/shard_map/dot_general | solution.py:84
  11.6 0.8 convolution_convert_fusion.4
  12.4 0.9 copy_bitcast_fusion
  13.3 0.9 copy.39
  15.7 1.2 subtract_convert_fusion
  17.7 0.9 fusion.38
  18.6 8.8 %conditional.2 = (f32[8,256]{1,0:T(8,128)}, f32[8,256]{1,0:T(8,128)S(1)}, f32[8,256,128]{2,1,0:T(8,128)S(1)}) conditional(s32[]{:T(128)} %convert_element_type.74, () %tuple.50, (s32[]{:T(128)}, s32[256]{0:T(256)S(1)}, s32[256]{0:T(256)S(1)}, bf16[256,512]{1,0:T(8,128)(2,1)}, bf16[512,1024]{1,0:T(8,128)(2,1)S(1)}, ...), branch_computations={%region_2.0_spmd, %region_3.6_spmd} | conditional | flops 877601024 | bytes 17297436 | solution.py:128
  18.6 1.4 fusion.6
  20.6 1.5 fusion.44
  22.7 1.0 fusion.5
  24.4 1.4 fusion.7
  25.8 1.5 convolution_add_fusion
  27.4 1.0 copy-done.4
  28.3 106.0 %while.27 = (s32[]{:T(128)}, bf16[256,512]{1,0:T(8,128)(2,1)}, bf16[256,64]{0,1:T(8,128)(2,1)S(1)}, f32[8,256]{1,0:T(8,128)}, f32[8,256]{1,0:T(8,128)S(1)}, /*in...) while((s32[]{:T(128)}, bf16[256,512]{1,0:T(8,128)(2,1)}, ...), condition=%wide.region_11.12_spmd.clone.clone, body=%wide.region_6.11_spmd.clone.clone.sunk | while | flops 877859328 | bytes 34840128 | solution.py:142
  28.4 1.9 collective-permute-start
  30.3 3.5 %collective-permute-start.1 = (bf16[256,64]{0,1:T(8,128)(2,1)S(1)}, bf16[256,64]{0,1:T(8,128)(2,1)S(1)}, u32[]{:S(2)}, u32[]{:S(2)}) collective-permute-start(bf16[256,64]{0,1:T(8,128)(2,1)S(1)} %get-tuple-element.817), channel_id=1, source_target_pairs={{0,2},{2,4},{4,6},{6,8},{8,10},{10,12},{12,14},{14,16},{16,18},{18... | collective-permute-start | bytes 98312 | tf_op jit(solution)/shard_map/while/body/eval_jaxpr/ppermute | solution.py:21
  34.4 3.0 %collective-permute-done.1 = bf16[256,64]{0,1:T(8,128)(2,1)S(1)} collective-permute-done((bf16[256,64]{0,1:T(8,128)(2,1)S(1)}, bf16[256,64]{0,1:T(8,128)(2,1)S(1)}, u32[]{:S(2)}, u32[]{:S(2)}) %collective-permute-start.1) | collective-permute-done | bytes 32800 | tf_op jit(solution)/shard_map/while/body/eval_jaxpr/ppermute | solution.py:21
  37.5 7.8 %conditional.6 = ((f32[8,256]{1,0:T(8,128)}, f32[8,256]{1,0:T(8,128)S(1)}, f32[8,256,128]{2,1,0:T(8,128)})) conditional(s32[]{:T(128)} %convert_element_type.126, (f32[8,256]{1,0:T(8,128)}, f32[8,256]{1,0:T(8,128)S(1)}, f32[8,256,128]{2,1,0:T(8,128)}) %tuple.88, (s32[]{:T(128)}, s32[256]{0:T(256)S(1)}, s32[]{:T(128)}, ...), branch_computations={%region_7.7_spmd, %region_8.10_spmd} | conditional | flops 877859328 | bytes 33069208 | solution.py:128
  39.0 1.5 fusion.45
  40.6 0.8 max.2
  42.9 0.9 convolution_add_fusion.1
  43.8 1.0 copy-done.6
  46.1 1.9 collective-permute-start
  48.0 2.6 %collective-permute-start.1 = (bf16[256,64]{0,1:T(8,128)(2,1)S(1)}, bf16[256,64]{0,1:T(8,128)(2,1)S(1)}, u32[]{:S(2)}, u32[]{:S(2)}) collective-permute-start(bf16[256,64]{0,1:T(8,128)(2,1)S(1)} %get-tuple-element.817), channel_id=1, source_target_pairs={{0,2},{2,4},{4,6},{6,8},{8,10},{10,12},{12,14},{14,16},{16,18},{18... | collective-permute-start | bytes 98312 | tf_op jit(solution)/shard_map/while/body/eval_jaxpr/ppermute | solution.py:21
  51.3 3.9 %collective-permute-done.1 = bf16[256,64]{0,1:T(8,128)(2,1)S(1)} collective-permute-done((bf16[256,64]{0,1:T(8,128)(2,1)S(1)}, bf16[256,64]{0,1:T(8,128)(2,1)S(1)}, u32[]{:S(2)}, u32[]{:S(2)}) %collective-permute-start.1) | collective-permute-done | bytes 32800 | tf_op jit(solution)/shard_map/while/body/eval_jaxpr/ppermute | solution.py:21
  55.2 0.7 copy.84
  56.0 1.9 collective-permute-start
  57.9 9.5 %collective-permute-start.1 = (bf16[256,64]{0,1:T(8,128)(2,1)S(1)}, bf16[256,64]{0,1:T(8,128)(2,1)S(1)}, u32[]{:S(2)}, u32[]{:S(2)}) collective-permute-start(bf16[256,64]{0,1:T(8,128)(2,1)S(1)} %get-tuple-element.817), channel_id=1, source_target_pairs={{0,2},{2,4},{4,6},{6,8},{8,10},{10,12},{12,14},{14,16},{16,18},{18... | collective-permute-start | bytes 98312 | tf_op jit(solution)/shard_map/while/body/eval_jaxpr/ppermute | solution.py:21
  68.1 1.5 collective-permute-done.1
  69.6 0.7 copy.84
  70.3 1.9 collective-permute-start
  72.3 4.2 %collective-permute-start.1 = (bf16[256,64]{0,1:T(8,128)(2,1)S(1)}, bf16[256,64]{0,1:T(8,128)(2,1)S(1)}, u32[]{:S(2)}, u32[]{:S(2)}) collective-permute-start(bf16[256,64]{0,1:T(8,128)(2,1)S(1)} %get-tuple-element.817), channel_id=1, source_target_pairs={{0,2},{2,4},{4,6},{6,8},{8,10},{10,12},{12,14},{14,16},{16,18},{18... | collective-permute-start | bytes 98312 | tf_op jit(solution)/shard_map/while/body/eval_jaxpr/ppermute | solution.py:21
  77.1 6.8 %collective-permute-done.1 = bf16[256,64]{0,1:T(8,128)(2,1)S(1)} collective-permute-done((bf16[256,64]{0,1:T(8,128)(2,1)S(1)}, bf16[256,64]{0,1:T(8,128)(2,1)S(1)}, u32[]{:S(2)}, u32[]{:S(2)}) %collective-permute-start.1) | collective-permute-done | bytes 32800 | tf_op jit(solution)/shard_map/while/body/eval_jaxpr/ppermute | solution.py:21
  84.0 0.7 copy.84
  84.7 4.2 %collective-permute-start = (bf16[256,512]{1,0:T(8,128)(2,1)}, bf16[256,512]{1,0:T(8,128)(2,1)S(1)}, u32[]{:S(2)}, u32[]{:S(2)}) collective-permute-start(bf16[256,512]{1,0:T(8,128)(2,1)} %get-tuple-element.816), channel_id=1, source_target_pairs={{0,2},{2,4},{4,6},{6,8},{8,10},{10,12},{12,14},{14,16},{16,18},{18... | collective-permute-start | bytes 786440 | tf_op jit(solution)/shard_map/while/body/eval_jaxpr/ppermute | solution.py:21
  88.9 5.1 %collective-permute-start.1 = (bf16[256,64]{0,1:T(8,128)(2,1)S(1)}, bf16[256,64]{0,1:T(8,128)(2,1)S(1)}, u32[]{:S(2)}, u32[]{:S(2)}) collective-permute-start(bf16[256,64]{0,1:T(8,128)(2,1)S(1)} %get-tuple-element.817), channel_id=1, source_target_pairs={{0,2},{2,4},{4,6},{6,8},{8,10},{10,12},{12,14},{14,16},{16,18},{18... | collective-permute-start | bytes 98312 | tf_op jit(solution)/shard_map/while/body/eval_jaxpr/ppermute | solution.py:21
  94.7 5.3 %collective-permute-done.1 = bf16[256,64]{0,1:T(8,128)(2,1)S(1)} collective-permute-done((bf16[256,64]{0,1:T(8,128)(2,1)S(1)}, bf16[256,64]{0,1:T(8,128)(2,1)S(1)}, u32[]{:S(2)}, u32[]{:S(2)}) %collective-permute-start.1) | collective-permute-done | bytes 32800 | tf_op jit(solution)/shard_map/while/body/eval_jaxpr/ppermute | solution.py:21
  100.7 1.9 collective-permute-start
  102.6 9.1 %collective-permute-start.1 = (bf16[256,64]{0,1:T(8,128)(2,1)S(1)}, bf16[256,64]{0,1:T(8,128)(2,1)S(1)}, u32[]{:S(2)}, u32[]{:S(2)}) collective-permute-start(bf16[256,64]{0,1:T(8,128)(2,1)S(1)} %get-tuple-element.817), channel_id=1, source_target_pairs={{0,2},{2,4},{4,6},{6,8},{8,10},{10,12},{12,14},{14,16},{16,18},{18... | collective-permute-start | bytes 98312 | tf_op jit(solution)/shard_map/while/body/eval_jaxpr/ppermute | solution.py:21
  112.4 4.4 %collective-permute-done.1 = bf16[256,64]{0,1:T(8,128)(2,1)S(1)} collective-permute-done((bf16[256,64]{0,1:T(8,128)(2,1)S(1)}, bf16[256,64]{0,1:T(8,128)(2,1)S(1)}, u32[]{:S(2)}, u32[]{:S(2)}) %collective-permute-start.1) | collective-permute-done | bytes 32800 | tf_op jit(solution)/shard_map/while/body/eval_jaxpr/ppermute | solution.py:21
  117.5 1.9 collective-permute-start
  119.5 2.2 collective-permute-start.1
  122.3 11.3 %collective-permute-done.1 = bf16[256,64]{0,1:T(8,128)(2,1)S(1)} collective-permute-done((bf16[256,64]{0,1:T(8,128)(2,1)S(1)}, bf16[256,64]{0,1:T(8,128)(2,1)S(1)}, u32[]{:S(2)}, u32[]{:S(2)}) %collective-permute-start.1) | collective-permute-done | bytes 32800 | tf_op jit(solution)/shard_map/while/body/eval_jaxpr/ppermute | solution.py:21
  134.4 7.4 %fusion.32 = bf16[256,4096]{1,0:T(8,128)(2,1)} fusion(bf16[8,128,4096]{2,1,0:T(8,128)(2,1)} %bitcast.77, f32[8,256,128]{2,1,0:T(8,128)} %get-tuple-element.539, f32[8,256]{1,0:T(8,128)S(1)} %get-tuple-element.540), kind=kOutput, calls=%fused_computation.49 | convolution fusion | flops 2149056512 | bytes 11542528 | tf_op jit(solution)/shard_map/hqd,hdm->qm/dot_general | solution.py:146
  141.8 70.3 %all-reduce.2.cloned.1.call-done = bf16[256,4096]{1,0:T(8,128)(2,1)} async-done(((bf16[256,4096]{1,0:T(8,128)(2,1)}), bf16[256,4096]{1,0:T(8,128)(2,1)}) %all-reduce.2.cloned.1.call-update) | async-done | bytes 2097168 | tf_op jit(solution)/shard_map/psum | solution.py:150
  212.2 3.1 %copy.90 = bf16[256,4096]{1,0:T(8,128)(2,1)} copy(bf16[256,4096]{1,0:T(8,128)(2,1)} %all-reduce.2.cloned.1.call-done) | data formatting | bytes 4194304
  (81 shorter events, 10.2 us)
Async XLA Ops:
  6.5 5.0 %copy-start = (bf16[1024,1024]{1,0:T(8,128)(2,1)S(1)}, bf16[1024,1024]{1,0:T(8,128)(2,1)}, u32[]{:S(2)}) copy-start(bf16[1024,1024]{1,0:T(8,128)(2,1)} %param.23) | copy-start | bytes 6291460
  6.5 5.0 %copy-start.10 = (bf16[256,1024]{1,0:T(8,128)(2,1)S(1)}, bf16[256,1024]{1,0:T(8,128)(2,1)}, u32[]{:S(2)}) copy-start(bf16[256,1024]{1,0:T(8,128)(2,1)} %param.17) | copy-start | bytes 1572868
  6.5 5.0 %copy-start.13 = (f32[1024]{0:T(1024)S(1)}, f32[1024]{0:T(1024)}, u32[]{:S(2)}) copy-start(f32[1024]{0:T(1024)} %param.21) | copy-start | bytes 12292
  6.5 205.6 %all-reduce.2.cloned.1.call-start = ((), (), s32[]{:S(2)}) async-start(), calls=%async_computation | async-start | bytes 4194304 | tf_op jit(solution)/shard_map/psum | solution.py:150
  11.5 2.6 %copy-start.9 = (bf16[256,512]{1,0:T(8,128)(2,1)S(1)}, bf16[256,512]{1,0:T(8,128)(2,1)}, u32[]{:S(2)}) copy-start(bf16[256,512]{1,0:T(8,128)(2,1)} %param.18) | copy-start | bytes 786436
  12.3 2.0 copy-start.11
  12.3 5.4 %copy-start.12 = (f32[512]{0:T(512)S(1)}, f32[512]{0:T(512)}, u32[]{:S(2)}) copy-start(f32[512]{0:T(512)} %param.22) | copy-start | bytes 6148
  12.4 6.2 %copy-start.1 = (bf16[512,1024]{1,0:T(8,128)(2,1)S(1)}, bf16[512,1024]{1,0:T(8,128)(2,1)}, u32[]{:S(2)}) copy-start(bf16[512,1024]{1,0:T(8,128)(2,1)} %param.25) | copy-start | bytes 3145732
  15.5 3.1 %copy-start.2 = (bf16[512,1024]{1,0:T(8,128)(2,1)S(1)}, bf16[512,1024]{1,0:T(8,128)(2,1)}, u32[]{:S(2)}) copy-start(bf16[512,1024]{1,0:T(8,128)(2,1)} %param.26) | copy-start | bytes 3145732
  15.5 3.1 %copy-start.8 = (bf16[32,8,8,128]{3,2,1,0:T(8,128)(2,1)S(1)}, bf16[32,8,8,128]{3,2,1,0:T(8,128)(2,1)}, u32[]{:S(2)}) copy-start(bf16[32,8,8,128]{3,2,1,0:T(8,128)(2,1)} %copy.39) | copy-start | bytes 1572868
  27.4 1.0 copy-start.4
  28.4 9.1 %collective-permute-start = (bf16[256,512]{1,0:T(8,128)(2,1)}, bf16[256,512]{1,0:T(8,128)(2,1)S(1)}, u32[]{:S(2)}, u32[]{:S(2)}) collective-permute-start(bf16[256,512]{1,0:T(8,128)(2,1)} %get-tuple-element.816), channel_id=1, source_target_pairs={{0,2},{2,4},{4,6},{6,8},{8,10},{10,12},{12,14},{14,16},{16,18},{18... | collective-permute-start | bytes 786440 | tf_op jit(solution)/shard_map/while/body/eval_jaxpr/ppermute | solution.py:21
  30.3 7.2 %collective-permute-start.1 = (bf16[256,64]{0,1:T(8,128)(2,1)S(1)}, bf16[256,64]{0,1:T(8,128)(2,1)S(1)}, u32[]{:S(2)}, u32[]{:S(2)}) collective-permute-start(bf16[256,64]{0,1:T(8,128)(2,1)S(1)} %get-tuple-element.817), channel_id=1, source_target_pairs={{0,2},{2,4},{4,6},{6,8},{8,10},{10,12},{12,14},{14,16},{16,18},{18... | collective-permute-start | bytes 98312 | tf_op jit(solution)/shard_map/while/body/eval_jaxpr/ppermute | solution.py:21
  37.5 1.0 copy-start.7
  40.5 1.9 copy-start.3
  40.5 2.3 %copy-start.5 = (f32[8,256,128]{2,1,0:T(8,128)S(1)}, f32[8,256,128]{2,1,0:T(8,128)}, u32[]{:S(2)}) copy-start(f32[8,256,128]{2,1,0:T(8,128)} %get-tuple-element.511) | copy-start | bytes 3145732 | tf_op jit(solution)/shard_map/while/body/eval_jaxpr/cond
  43.8 1.0 copy-start.6
  46.1 9.1 %collective-permute-start = (bf16[256,512]{1,0:T(8,128)(2,1)}, bf16[256,512]{1,0:T(8,128)(2,1)S(1)}, u32[]{:S(2)}, u32[]{:S(2)}) collective-permute-start(bf16[256,512]{1,0:T(8,128)(2,1)} %get-tuple-element.816), channel_id=1, source_target_pairs={{0,2},{2,4},{4,6},{6,8},{8,10},{10,12},{12,14},{14,16},{16,18},{18... | collective-permute-start | bytes 786440 | tf_op jit(solution)/shard_map/while/body/eval_jaxpr/ppermute | solution.py:21
  48.0 7.2 %collective-permute-start.1 = (bf16[256,64]{0,1:T(8,128)(2,1)S(1)}, bf16[256,64]{0,1:T(8,128)(2,1)S(1)}, u32[]{:S(2)}, u32[]{:S(2)}) collective-permute-start(bf16[256,64]{0,1:T(8,128)(2,1)S(1)} %get-tuple-element.817), channel_id=1, source_target_pairs={{0,2},{2,4},{4,6},{6,8},{8,10},{10,12},{12,14},{14,16},{16,18},{18... | collective-permute-start | bytes 98312 | tf_op jit(solution)/shard_map/while/body/eval_jaxpr/ppermute | solution.py:21
  56.0 13.6 %collective-permute-start = (bf16[256,512]{1,0:T(8,128)(2,1)}, bf16[256,512]{1,0:T(8,128)(2,1)S(1)}, u32[]{:S(2)}, u32[]{:S(2)}) collective-permute-start(bf16[256,512]{1,0:T(8,128)(2,1)} %get-tuple-element.816), channel_id=1, source_target_pairs={{0,2},{2,4},{4,6},{6,8},{8,10},{10,12},{12,14},{14,16},{16,18},{18... | collective-permute-start | bytes 786440 | tf_op jit(solution)/shard_map/while/body/eval_jaxpr/ppermute | solution.py:21
  57.9 11.7 %collective-permute-start.1 = (bf16[256,64]{0,1:T(8,128)(2,1)S(1)}, bf16[256,64]{0,1:T(8,128)(2,1)S(1)}, u32[]{:S(2)}, u32[]{:S(2)}) collective-permute-start(bf16[256,64]{0,1:T(8,128)(2,1)S(1)} %get-tuple-element.817), channel_id=1, source_target_pairs={{0,2},{2,4},{4,6},{6,8},{8,10},{10,12},{12,14},{14,16},{16,18},{18... | collective-permute-start | bytes 98312 | tf_op jit(solution)/shard_map/while/body/eval_jaxpr/ppermute | solution.py:21
  70.3 13.6 %collective-permute-start = (bf16[256,512]{1,0:T(8,128)(2,1)}, bf16[256,512]{1,0:T(8,128)(2,1)S(1)}, u32[]{:S(2)}, u32[]{:S(2)}) collective-permute-start(bf16[256,512]{1,0:T(8,128)(2,1)} %get-tuple-element.816), channel_id=1, source_target_pairs={{0,2},{2,4},{4,6},{6,8},{8,10},{10,12},{12,14},{14,16},{16,18},{18... | collective-permute-start | bytes 786440 | tf_op jit(solution)/shard_map/while/body/eval_jaxpr/ppermute | solution.py:21
  72.3 11.7 %collective-permute-start.1 = (bf16[256,64]{0,1:T(8,128)(2,1)S(1)}, bf16[256,64]{0,1:T(8,128)(2,1)S(1)}, u32[]{:S(2)}, u32[]{:S(2)}) collective-permute-start(bf16[256,64]{0,1:T(8,128)(2,1)S(1)} %get-tuple-element.817), channel_id=1, source_target_pairs={{0,2},{2,4},{4,6},{6,8},{8,10},{10,12},{12,14},{14,16},{16,18},{18... | collective-permute-start | bytes 98312 | tf_op jit(solution)/shard_map/while/body/eval_jaxpr/ppermute | solution.py:21
  84.7 15.3 %collective-permute-start = (bf16[256,512]{1,0:T(8,128)(2,1)}, bf16[256,512]{1,0:T(8,128)(2,1)S(1)}, u32[]{:S(2)}, u32[]{:S(2)}) collective-permute-start(bf16[256,512]{1,0:T(8,128)(2,1)} %get-tuple-element.816), channel_id=1, source_target_pairs={{0,2},{2,4},{4,6},{6,8},{8,10},{10,12},{12,14},{14,16},{16,18},{18... | collective-permute-start | bytes 786440 | tf_op jit(solution)/shard_map/while/body/eval_jaxpr/ppermute | solution.py:21
  88.9 11.0 %collective-permute-start.1 = (bf16[256,64]{0,1:T(8,128)(2,1)S(1)}, bf16[256,64]{0,1:T(8,128)(2,1)S(1)}, u32[]{:S(2)}, u32[]{:S(2)}) collective-permute-start(bf16[256,64]{0,1:T(8,128)(2,1)S(1)} %get-tuple-element.817), channel_id=1, source_target_pairs={{0,2},{2,4},{4,6},{6,8},{8,10},{10,12},{12,14},{14,16},{16,18},{18... | collective-permute-start | bytes 98312 | tf_op jit(solution)/shard_map/while/body/eval_jaxpr/ppermute | solution.py:21
  100.7 16.1 %collective-permute-start = (bf16[256,512]{1,0:T(8,128)(2,1)}, bf16[256,512]{1,0:T(8,128)(2,1)S(1)}, u32[]{:S(2)}, u32[]{:S(2)}) collective-permute-start(bf16[256,512]{1,0:T(8,128)(2,1)} %get-tuple-element.816), channel_id=1, source_target_pairs={{0,2},{2,4},{4,6},{6,8},{8,10},{10,12},{12,14},{14,16},{16,18},{18... | collective-permute-start | bytes 786440 | tf_op jit(solution)/shard_map/while/body/eval_jaxpr/ppermute | solution.py:21
  102.6 14.1 %collective-permute-start.1 = (bf16[256,64]{0,1:T(8,128)(2,1)S(1)}, bf16[256,64]{0,1:T(8,128)(2,1)S(1)}, u32[]{:S(2)}, u32[]{:S(2)}) collective-permute-start(bf16[256,64]{0,1:T(8,128)(2,1)S(1)} %get-tuple-element.817), channel_id=1, source_target_pairs={{0,2},{2,4},{4,6},{6,8},{8,10},{10,12},{12,14},{14,16},{16,18},{18... | collective-permute-start | bytes 98312 | tf_op jit(solution)/shard_map/while/body/eval_jaxpr/ppermute | solution.py:21
  117.5 16.1 %collective-permute-start = (bf16[256,512]{1,0:T(8,128)(2,1)}, bf16[256,512]{1,0:T(8,128)(2,1)S(1)}, u32[]{:S(2)}, u32[]{:S(2)}) collective-permute-start(bf16[256,512]{1,0:T(8,128)(2,1)} %get-tuple-element.816), channel_id=1, source_target_pairs={{0,2},{2,4},{4,6},{6,8},{8,10},{10,12},{12,14},{14,16},{16,18},{18... | collective-permute-start | bytes 786440 | tf_op jit(solution)/shard_map/while/body/eval_jaxpr/ppermute | solution.py:21
  119.5 14.1 %collective-permute-start.1 = (bf16[256,64]{0,1:T(8,128)(2,1)S(1)}, bf16[256,64]{0,1:T(8,128)(2,1)S(1)}, u32[]{:S(2)}, u32[]{:S(2)}) collective-permute-start(bf16[256,64]{0,1:T(8,128)(2,1)S(1)} %get-tuple-element.817), channel_id=1, source_target_pairs={{0,2},{2,4},{4,6},{6,8},{8,10},{10,12},{12,14},{14,16},{16,18},{18... | collective-permute-start | bytes 98312 | tf_op jit(solution)/shard_map/while/body/eval_jaxpr/ppermute | solution.py:21
Sparse Core Ops, SparseCore 0:
  142.0 70.1 all-reduce.1
where the time goes:
time: 226 us; the launch traced here: 222 us
  waiting for transfers between devices  107 us (47%)
  starting transfers between devices  52 us (23%)
  matrix products  21 us (9%)
  between operations  14.2 us (6%)
  local copies, waits for them, and re-layouts  13.7 us (6%)
  other arithmetic  9.73 us (4%)
  loops' own time  5.01 us (2%)
    psum x1, waiting for transfers between devices, on_device(): mixed = lax.psum(group_term.astype(jnp.bfloat16), 'tp')  70.3 us
    ppermute x14, starting transfers between devices, from_behind(): lax.ppermute(value, axis, [(source, source + steps) for source in range(i...  52 us
    ppermute x14, waiting for transfers between devices, from_behind(): lax.ppermute(value, axis, [(source, source + steps) for source in range(i...  36.2 us
    dot_general x1, matrix products, on_device(): jnp.einsum('hqd,hdm->qm', attended, weight_heads, preferred_element_type=...  7.45 us
    unnamed x23, local copies, waits for them, and re-layouts  5.95 us
    while x14, local copies, waits for them, and re-layouts  5.16 us
    another operation x1, loops' own time, on_device(): lax.fori_loop(0, SPAN - 1, advance, (payload, softmax_state))  4.73 us
  transfers between devices with their start and end apart: 15, of which 8 were waited for; matrix products, arithmetic and copies ran while one was open for 0% of the time, Pallas kernels for 0%

commit v1 on v0

v1 whole, which is shorter than its diff:
```python
import functools

import jax
import jax.numpy as jnp
import numpy as np
from jax import lax
from jax.experimental import pallas as pl
from jax.experimental.pallas import tpu as pltpu
from jax.sharding import PartitionSpec as P

CONTENT = 128
ROTARY = 64
SPAN = 8
LANES = 128
CHUNKS = 4

norm_eps = 1e-06
rope_theta = 10000.0
masked_score = -1e30
MESH = pl.DeviceIdType.MESH


def rms_scale(latent, scaling):
    entries = latent.astype(jnp.float32)
    scaled = entries * lax.rsqrt(jnp.mean(entries * entries, axis=-1, keepdims=True) + norm_eps)
    return (scaled * scaling).astype(jnp.bfloat16)


def kernel(
    sp_size,
    tp_size,
    query_ref,
    shared_ref,
    rotary_ref,
    start_ref,
    query_gain_ref,
    shared_gain_ref,
    frequency_ref,
    content_hbm,
    rotary_hbm,
    key_hbm,
    value_hbm,
    output_hbm,
    mixed_hbm,
    content_w,
    rotary_w,
    key_w,
    value_w,
    output_w,
    halo,
    keys,
    values,
    turns,
    queries,
    query_rows,
    cosines,
    sines,
    bias,
    attended,
    terms,
    landed,
    load_sems,
    halo_recv,
    halo_send,
    term_recv,
    term_send,
    store_sems,
):
    length = query_ref.shape[0]
    shared_rank = shared_ref.shape[1]
    heads = keys.shape[0]
    fold = length * ROTARY // shared_rank
    window = SPAN * length
    rows = length // CHUNKS
    me = lax.axis_index("sp")
    my_tp = lax.axis_index("tp")
    chips = sp_size // 2
    chip = me // 2
    core = me % 2
    odd = chip % 2 == 1
    partner = me + 1 - 2 * core
    beside = me + 2 - 4 * (chip % 2)
    ahead = me + 4
    has_ahead = chip + 2 < chips
    has_behind = chip >= 2

    loads = [
        pltpu.make_async_copy(source, target, load_sems.at[n])
        for n, (source, target) in enumerate(
            (
                (content_hbm, content_w),
                (rotary_hbm, rotary_w),
                (key_hbm, key_w),
                (value_hbm, value_w),
                (output_hbm, output_w),
            )
        )
    ]
    for load in loads:
        load.start()

    barrier = pltpu.get_barrier_semaphore()
    pl.semaphore_signal(barrier, inc=1, device_id={"sp": partner}, device_id_type=MESH)
    pl.semaphore_signal(barrier, inc=1, device_id={"sp": beside}, device_id_type=MESH)
    for step in range(1, tp_size):
        pl.semaphore_signal(
            barrier, inc=1, device_id={"tp": (my_tp + step) % tp_size}, device_id_type=MESH
        )

    @pl.when(has_ahead)
    def _():
        pl.semaphore_signal(barrier, inc=1, device_id={"sp": ahead}, device_id_type=MESH)

    @pl.when(has_behind)
    def _():
        pl.semaphore_signal(barrier, inc=1, device_id={"sp": me - 4}, device_id_type=MESH)

    lane = lax.broadcasted_iota(jnp.int32, (length, LANES), 1)
    first_half = lane % ROTARY < ROTARY // 2
    low_lanes = lane < ROTARY
    places = (me * length + lax.broadcasted_iota(jnp.int32, (length, LANES), 0)).astype(jnp.float32)
    angles = places * frequency_ref[...]
    cosines[...] = jnp.cos(angles)
    sine = jnp.sin(angles)
    sines[...] = jnp.where(first_half, -sine, sine)

    def rotate(entries):
        swapped = jnp.where(
            first_half,
            pltpu.roll(entries, LANES - ROTARY // 2, 1),
            pltpu.roll(entries, ROTARY // 2, 1),
        )
        return entries * cosines[...] + swapped * sines[...]

    halo[0, :length, :] = rms_scale(shared_ref[...], shared_gain_ref[...])
    raw_key = rotary_ref[...].astype(jnp.float32)
    turned = rotate(jnp.concatenate([raw_key, raw_key], axis=1))
    for j in range(shared_rank // LANES):
        upper = turned[2 * j * fold : (2 * j + 1) * fold]
        lower = turned[(2 * j + 1) * fold : (2 * j + 2) * fold]
        halo[0, length:, j * LANES : (j + 1) * LANES] = jnp.where(
            low_lanes[:fold], upper, lower
        ).astype(jnp.bfloat16)

    pl.semaphore_wait(
        barrier, 1 + tp_size + has_ahead.astype(jnp.int32) + has_behind.astype(jnp.int32)
    )

    def send(n, source, target, device):
        return pltpu.make_async_remote_copy(
            src_ref=halo.at[source],
            dst_ref=halo.at[target],
            send_sem=halo_send.at[n],
            recv_sem=halo_recv.at[target],
            device_id={"sp": device},
            device_id_type=MESH,
        )

    even = jnp.logical_not(odd)
    first_core = core == 0
    second_core = core == 1
    have = lambda slot: me >= slot
    sends = [
        (0, has_ahead, send(0, 0, 4, ahead)),
        (0, even, send(1, 0, 2, beside)),
        (0, first_core, send(2, 0, 1, partner)),
        (4, has_behind & has_ahead & (odd | second_core), send(3, 4, 8, ahead)),
        (4, has_behind & even, send(4, 4, 6, beside)),
        (4, has_behind & odd, send(5, 4, 2, beside)),
        (4, has_behind & first_core, send(6, 4, 5, partner)),
        (4, has_behind & second_core, send(7, 4, 3, partner)),
        (2, have(2) & first_core, send(8, 2, 3, partner)),
        (2, have(2) & second_core, send(9, 2, 1, partner)),
        (8, have(8) & odd, send(10, 8, 6, beside)),
        (8, have(8) & second_core, send(11, 8, 7, partner)),
        (6, have(6) & first_core, send(12, 6, 7, partner)),
        (6, have(6) & second_core, send(13, 6, 5, partner)),
    ]

    def start_from(slot):
        for source, condition, copy in sends:
            if source == slot:

                @pl.when(condition)
                def _(copy=copy):
                    copy.start()

    def await_slot(slot):
        expected = have(slot)
        if slot == 8:
            expected = expected & (odd | second_core)

        @pl.when(expected)
        def _():
            pltpu.make_async_copy(halo.at[slot], halo.at[slot], halo_recv.at[slot]).wait()

        if slot < SPAN:

            @pl.when(jnp.logical_not(expected))
            def _():
                halo[slot] = jnp.zeros(halo.shape[1:], halo.dtype)

    def expand(slot):
        base = (SPAN - 1 - slot) * length
        for j in range(shared_rank // LANES):
            piece = halo[slot, length:, j * LANES : (j + 1) * LANES].astype(jnp.float32)
            flipped = pltpu.roll(piece, ROTARY, 1)
            mask = low_lanes[:fold]
            place = base + 2 * j * fold
            turns[place : place + fold, :] = jnp.where(mask, piece, flipped).astype(jnp.bfloat16)
            turns[place + fold : place + 2 * fold, :] = jnp.where(mask, flipped, piece).astype(
                jnp.bfloat16
            )

        def pair(j, carry):
            columns = pl.ds(pl.multiple_of(j * 2 * LANES, 2 * LANES), 2 * LANES)
            block = halo[slot, :length, :]
            for weight, target in ((key_w, keys), (value_w, values)):
                result = jnp.dot(
                    block, weight[:, columns], preferred_element_type=jnp.float32
                ).astype(jnp.bfloat16)
                target[2 * j, base : base + length, :] = result[:, :LANES]
                target[2 * j + 1, base : base + length, :] = result[:, LANES:]
            return carry

        lax.fori_loop(0, heads // 2, pair, 0)

    start_from(0)

    query_rows[...] = rms_scale(query_ref[...], query_gain_ref[...])
    loads[0].wait()
    loads[1].wait()

    def project(j, carry):
        columns = pl.ds(pl.multiple_of(j * 2 * LANES, 2 * LANES), 2 * LANES)
        content = jnp.dot(
            query_rows[...], content_w[:, columns], preferred_element_type=jnp.float32
        ).astype(jnp.bfloat16)
        narrow = pl.ds(pl.multiple_of(j * LANES, LANES), LANES)
        turned = rotate(
            jnp.dot(query_rows[...], rotary_w[:, narrow], preferred_element_type=jnp.float32)
        )
        queries[2 * j, :, :LANES] = content[:, :LANES]
        queries[2 * j + 1, :, :LANES] = content[:, LANES:]
        queries[2 * j, :, LANES:] = jnp.where(low_lanes, turned, 0.0).astype(jnp.bfloat16)
        queries[2 * j + 1, :, LANES:] = jnp.where(low_lanes, 0.0, turned).astype(jnp.bfloat16)
        return carry

    lax.fori_loop(0, heads // 2, project, 0)
    loads[2].wait()
    loads[3].wait()
    expand(0)
    for slot in (4, 2):
        await_slot(slot)
        start_from(slot)
    expand(4)
    await_slot(1)
    expand(2)
    expand(1)
    for slot in (8, 6):
        await_slot(slot)
        start_from(slot)
    expand(6)
    for slot in (3, 5, 7):
        await_slot(slot)
        expand(slot)
    loads[4].wait()

    factor = (CONTENT + ROTARY) ** (-0.5) * 1.4426950408889634
    opening = (me - (SPAN - 1)) * length

    def term_copy(chunk, step):
        place = pl.ds(pl.multiple_of(chunk * rows, rows), rows)
        return pltpu.make_async_remote_copy(
            src_ref=terms.at[place],
            dst_ref=landed.at[step - 1, place],
            send_sem=term_send.at[step - 1, chunk],
            recv_sem=term_recv.at[step - 1, chunk],
            device_id={"tp": (my_tp + step) % tp_size},
            device_id_type=MESH,
        )

    def attend(chunk, carry):
        offset = pl.multiple_of(chunk * rows, rows)
        place = pl.ds(offset, rows)
        key_places = opening + lax.broadcasted_iota(jnp.int32, (rows, window), 1)
        query_places = me * length + offset + lax.broadcasted_iota(jnp.int32, (rows, window), 0)
        visible = (key_places >= start_ref[place, :]) & (key_places <= query_places)
        bias[...] = jnp.where(visible, 0.0, masked_score)

        def one_head(h, inner):
            held = jnp.concatenate([keys[h], turns[...]], axis=1)
            scores = lax.dot_general(
                queries[h, place, :],
                held,
                (((1,), (1,)), ((), ())),
                preferred_element_type=jnp.float32,
            )
            scores = scores + bias[...]
            highest = jnp.max(scores, axis=-1, keepdims=True)
            weights = jnp.exp2((scores - highest) * factor)
            denominator = jnp.sum(weights, axis=-1, keepdims=True)
            summed = jnp.dot(
                weights.astype(jnp.bfloat16), values[h], preferred_element_type=jnp.float32
            )
            attended[:, pl.ds(pl.multiple_of(h * LANES, LANES), LANES)] = (
                summed / denominator
            ).astype(jnp.bfloat16)
            return inner

        lax.fori_loop(0, heads, one_head, 0)
        wide = 4 * LANES

        def output_columns(j, inner):
            columns = pl.ds(pl.multiple_of(j * wide, wide), wide)
            terms[place, columns] = jnp.dot(
                attended[...], output_w[:, columns], preferred_element_type=jnp.float32
            ).astype(jnp.bfloat16)
            return inner

        lax.fori_loop(0, output_w.shape[1] // wide, output_columns, 0)
        for step in range(1, tp_size):
            term_copy(chunk, step).start()
        return carry

    lax.fori_loop(0, CHUNKS, attend, 0)

    def store_copy(chunk):
        place = pl.ds(pl.multiple_of(chunk * rows, rows), rows)
        return pltpu.make_async_copy(landed.at[0, place], mixed_hbm.at[place], store_sems.at[chunk])

    def finish(chunk, carry):
        place = pl.ds(pl.multiple_of(chunk * rows, rows), rows)
        for step in range(1, tp_size):
            term_copy(chunk, step).wait_recv()
        total = terms[place, :].astype(jnp.float32)
        for step in range(1, tp_size):
            total = total + landed[step - 1, place, :].astype(jnp.float32)
        landed[0, place, :] = total.astype(jnp.bfloat16)
        store_copy(chunk).start()
        return carry

    lax.fori_loop(0, CHUNKS, finish, 0)
    for source, condition, copy in sends:

        @pl.when(condition)
        def _(copy=copy):
            copy.wait_send()

    def drain(chunk, carry):
        for step in range(1, tp_size):
            term_copy(chunk, step).wait_send()
        store_copy(chunk).wait()
        return carry

    lax.fori_loop(0, CHUNKS, drain, 0)


def on_device(
    query_latent,
    shared_latent,
    rotary_key,
    document_start,
    query_gain,
    shared_gain,
    content_weight,
    rotary_weight,
    key_weight,
    value_weight,
    output_weight,
):
    length, query_rank = query_latent.shape
    shared_rank = shared_latent.shape[1]
    sp_size = lax.axis_size("sp")
    tp_size = lax.axis_size("tp")
    heads = key_weight.shape[1] // CONTENT
    model = output_weight.shape[1]
    window = SPAN * length
    half = np.arange(0, ROTARY, 2, dtype=np.float32) / np.float32(ROTARY)
    frequency = (1.0 / np.power(np.float32(rope_theta), half)).astype(np.float32)
    frequency = jnp.asarray(np.tile(frequency, LANES // (ROTARY // 2))[None, :])
    fold = length * ROTARY // shared_rank
    low = jnp.bfloat16
    vmem = pl.BlockSpec(memory_space=pltpu.VMEM)
    hbm = pl.BlockSpec(memory_space=pl.ANY)
    return pl.pallas_call(
        functools.partial(kernel, sp_size, tp_size),
        out_shape=jax.ShapeDtypeStruct((length, model), low),
        in_specs=[vmem] * 7 + [hbm] * 5,
        out_specs=hbm,
        scratch_shapes=[
            pltpu.VMEM(content_weight.shape, low),
            pltpu.VMEM(rotary_weight.shape, low),
            pltpu.VMEM(key_weight.shape, low),
            pltpu.VMEM(value_weight.shape, low),
            pltpu.VMEM(output_weight.shape, low),
            pltpu.VMEM((SPAN + 1, length + fold, shared_rank), low),
            pltpu.VMEM((heads, window, LANES), low),
            pltpu.VMEM((heads, window, LANES), low),
            pltpu.VMEM((window, LANES), low),
            pltpu.VMEM((heads, length, 2 * LANES), low),
            pltpu.VMEM((length, query_rank), low),
            pltpu.VMEM((length, LANES), jnp.float32),
            pltpu.VMEM((length, LANES), jnp.float32),
            pltpu.VMEM((length // CHUNKS, window), jnp.float32),
            pltpu.VMEM((length // CHUNKS, heads * LANES), low),
            pltpu.VMEM((length, model), low),
            pltpu.VMEM((max(tp_size - 1, 1), length, model), low),
            pltpu.SemaphoreType.DMA((5,)),
            pltpu.SemaphoreType.DMA((SPAN + 1,)),
            pltpu.SemaphoreType.DMA((14,)),
            pltpu.SemaphoreType.DMA((max(tp_size - 1, 1), CHUNKS)),
            pltpu.SemaphoreType.DMA((max(tp_size - 1, 1), CHUNKS)),
            pltpu.SemaphoreType.DMA((CHUNKS,)),
        ],
        compiler_params=pltpu.CompilerParams(
            collective_id=0, has_side_effects=True, vmem_limit_bytes=60 * 1024 * 1024
        ),
    )(
        query_latent,
        shared_latent,
        rotary_key,
        document_start.reshape(length, 1),
        query_gain.reshape(1, query_rank),
        shared_gain.reshape(1, shared_rank),
        frequency,
        content_weight,
        rotary_weight,
        key_weight,
        value_weight,
        output_weight,
    )


def solution(mesh):
    return jax.shard_map(
        on_device,
        mesh=mesh,
        in_specs=(
            P("sp", None),
            P("sp", None),
            P("sp", None),
            P("sp"),
            P(),
            P(),
            P(None, "tp"),
            P(None, "tp"),
            P(None, "tp"),
            P(None, "tp"),
            P("tp", None),
        ),
        out_specs=P("sp", None),
        check_vma=False,
    )
```

time: 226 us -> 91 us (0.40); the launches traced: 222 us -> 90.7 us
  waiting for transfers between devices: 107 us -> 0 us
  Pallas kernels: 0 us -> 84.7 us
  starting transfers between devices: 52 us -> 0 us
  matrix products: 21 us -> 0 us
  between operations: 14.2 us -> 0.01 us
  other arithmetic: 9.73 us -> 0 us
  local copies, waits for them, and re-layouts: 13.7 us -> 6.08 us
  loops' own time: 5.01 us -> 0 us
    pallas_call x0 -> x1, Pallas kernels: none -> 84.7 us  [on_device(): pl.pallas_call(functools.partial(kernel, sp_size, tp_size), out_shape=jax...]
    psum x1 -> x0, waiting for transfers between devices: 70.3 us -> none  [on_device(): mixed = lax.psum(group_term.astype(jnp.bfloat16), 'tp')]
    ppermute x14 -> x0, starting transfers between devices: 52 us -> none  [from_behind(): lax.ppermute(value, axis, [(source, source + steps) for source in range(i...]
    ppermute x14 -> x0, waiting for transfers between devices: 36.2 us -> none  [from_behind(): lax.ppermute(value, axis, [(source, source + steps) for source in range(i...]
    dot_general x13 -> x0, matrix products: 21 us -> none  [the longest x1 7.45 us: on_device(): jnp.einsum('hqd,hdm->qm', attended, weight_heads, preferred_element_type=...]
    while x14 -> x0, local copies, waits for them, and re-layouts: 5.16 us -> none
    another operation x9 -> x0, loops' own time: 5.01 us -> none  [the longest x1 4.73 us: on_device(): lax.fori_loop(0, SPAN - 1, advance, (payload, softmax_state))]
    reduce_sum x4 -> x0, other arithmetic: 2.65 us -> none  [the longest x2 1.35 us: rms_scale(): jnp.mean(entries * entries, axis=-1, keepdims=True) + norm_eps]
  transfers between devices with their start and end apart: 15 -> 0, of which waited for: 8 -> 0; matrix products, arithmetic and copies ran while one was open for 0% -> 0% of each run, Pallas kernels for 0% -> 0%
where the time goes in v1:
time: 91 us; the launch traced here: 90.7 us
  Pallas kernels  84.7 us (93%)
  local copies, waits for them, and re-layouts  6.08 us (7%)
    pallas_call x1, Pallas kernels, on_device(): pl.pallas_call(functools.partial(kernel, sp_size, tp_size), out_shape=jax...  84.7 us
    unnamed x2, local copies, waits for them, and re-layouts  4.61 us

profile of v1, /device:TPU:16, one launch (start us, length us, event | category | flops | bytes accessed | tf_op | source)
XLA Modules:
  0.0 90.7 jit_solution(4439527720755533923)
XLA Ops:
  0.0 1.5 %copy.14.rotary_ref = bf16[256,64]{1,0:T(8,128)(2,1)} copy(bf16[256,64]{0,1:T(8,128)(2,1)} %param.14) | data formatting | bytes 65536 | tf_op args[2]
  1.5 1.5 %copy.15.start_ref = s32[256,1]{1,0:T(8,128)} copy(s32[256,1]{0,1:T(1,128)} %bitcast.5) | data formatting | bytes 2048 | tf_op jit(solution)/shard_map/reshape | solution.py:423
  3.0 84.7 %shard_map.118 = bf16[256,4096]{1,0:T(8,128)(2,1)} custom-call(bf16[256,1024]{1,0:T(8,128)(2,1)} %query_ref.1, bf16[256,512]{1,0:T(8,128)(2,1)} %shared_ref.1, bf16[256,64]{1,0:T(8,128)(2,1)} %copy.14.rotary_ref, s32[256,1]{1,0:T(8,128)} %copy.15.start_ref, f32[1,1024]{1,0:T(1,128)} %bitcast.3, f32[1,512]{1,0:T(1,128)} %bitcast.4, ...), custom_call_target="tpu_custom_call" | custom-call | tf_op jit(solution)/shard_map/pallas_call | solution.py:386
  87.6 3.1 %copy.17 = bf16[256,4096]{1,0:T(8,128)(2,1)} copy(bf16[256,4096]{1,0:T(8,128)(2,1)} %shard_map.118) | data formatting | bytes 4194304

commit v2 on v1

--- a/solution.py
+++ b/solution.py
@@ -13,6 +13,7 @@
 SPAN = 8
 LANES = 128
 CHUNKS = 4
+PIECES = CHUNKS + 1
 
 norm_eps = 1e-06
 rope_theta = 10000.0
@@ -55,6 +56,7 @@
     query_rows,
     cosines,
     sines,
+    starts,
     bias,
     attended,
     terms,
@@ -134,7 +136,7 @@
 
     halo[0, :length, :] = rms_scale(shared_ref[...], shared_gain_ref[...])
     raw_key = rotary_ref[...].astype(jnp.float32)
-    turned = rotate(jnp.concatenate([raw_key, raw_key], axis=1))
+    turned = rotate(jnp.transpose(jnp.concatenate([raw_key, raw_key], axis=0)))
     for j in range(shared_rank // LANES):
         upper = turned[2 * j * fold : (2 * j + 1) * fold]
         lower = turned[(2 * j + 1) * fold : (2 * j + 2) * fold]
@@ -227,6 +229,8 @@
 
     start_from(0)
 
+    begin = jnp.broadcast_to(start_ref[...].astype(jnp.float32), (LANES, length))
+    starts[...] = jnp.transpose(begin).astype(jnp.int32)
     query_rows[...] = rms_scale(query_ref[...], query_gain_ref[...])
     loads[0].wait()
     loads[1].wait()
@@ -269,8 +273,14 @@
     factor = (CONTENT + ROTARY) ** (-0.5) * 1.4426950408889634
     opening = (me - (SPAN - 1)) * length
 
-    def term_copy(chunk, step):
-        place = pl.ds(pl.multiple_of(chunk * rows, rows), rows)
+    half = rows // 2
+    loops = ((0, 2, half, 0), (2, PIECES, rows, rows))
+
+    def place_of(piece, size, shift):
+        return pl.ds(pl.multiple_of(piece * size - shift, half), size)
+
+    def term_copy(chunk, step, size, shift):
+        place = place_of(chunk, size, shift)
         return pltpu.make_async_remote_copy(
             src_ref=terms.at[place],
             dst_ref=landed.at[step - 1, place],
@@ -280,13 +290,13 @@
             device_id_type=MESH,
         )
 
-    def attend(chunk, carry):
-        offset = pl.multiple_of(chunk * rows, rows)
-        place = pl.ds(offset, rows)
-        key_places = opening + lax.broadcasted_iota(jnp.int32, (rows, window), 1)
-        query_places = me * length + offset + lax.broadcasted_iota(jnp.int32, (rows, window), 0)
-        visible = (key_places >= start_ref[place, :]) & (key_places <= query_places)
-        bias[...] = jnp.where(visible, 0.0, masked_score)
+    def attend(size, shift, chunk, carry):
+        offset = pl.multiple_of(chunk * size - shift, half)
+        place = pl.ds(offset, size)
+        key_places = opening + lax.broadcasted_iota(jnp.int32, (size, window), 1)
+        query_places = me * length + offset + lax.broadcasted_iota(jnp.int32, (size, window), 0)
+        visible = (key_places >= starts[place, :1]) & (key_places <= query_places)
+        bias[:size, :] = jnp.where(visible, 0.0, masked_score)
 
         def one_head(h, inner):
             held = jnp.concatenate([keys[h], turns[...]], axis=1)
@@ -296,14 +306,14 @@
                 (((1,), (1,)), ((), ())),
                 preferred_element_type=jnp.float32,
             )
-            scores = scores + bias[...]
+            scores = scores + bias[:size, :]
             highest = jnp.max(scores, axis=-1, keepdims=True)
             weights = jnp.exp2((scores - highest) * factor)
             denominator = jnp.sum(weights, axis=-1, keepdims=True)
             summed = jnp.dot(
                 weights.astype(jnp.bfloat16), values[h], preferred_element_type=jnp.float32
             )
-            attended[:, pl.ds(pl.multiple_of(h * LANES, LANES), LANES)] = (
+            attended[:size, pl.ds(pl.multiple_of(h * LANES, LANES), LANES)] = (
                 summed / denominator
             ).astype(jnp.bfloat16)
             return inner
@@ -314,46 +324,49 @@
         def output_columns(j, inner):
             columns = pl.ds(pl.multiple_of(j * wide, wide), wide)
             terms[place, columns] = jnp.dot(
-                attended[...], output_w[:, columns], preferred_element_type=jnp.float32
+                attended[:size, :], output_w[:, columns], preferred_element_type=jnp.float32
             ).astype(jnp.bfloat16)
             return inner
 
         lax.fori_loop(0, output_w.shape[1] // wide, output_columns, 0)
         for step in range(1, tp_size):
-            term_copy(chunk, step).start()
+            term_copy(chunk, step, size, shift).start()
         return carry
 
-    lax.fori_loop(0, CHUNKS, attend, 0)
-
-    def store_copy(chunk):
-        place = pl.ds(pl.multiple_of(chunk * rows, rows), rows)
+    for low, high, size, shift in loops:
+        lax.fori_loop(low, high, functools.partial(attend, size, shift), 0)
+
+    def store_copy(chunk, size, shift):
+        place = place_of(chunk, size, shift)
         return pltpu.make_async_copy(landed.at[0, place], mixed_hbm.at[place], store_sems.at[chunk])
 
-    def finish(chunk, carry):
-        place = pl.ds(pl.multiple_of(chunk * rows, rows), rows)
+    def finish(size, shift, chunk, carry):
+        place = place_of(chunk, size, shift)
         for step in range(1, tp_size):
-            term_copy(chunk, step).wait_recv()
+            term_copy(chunk, step, size, shift).wait_recv()
         total = terms[place, :].astype(jnp.float32)
         for step in range(1, tp_size):
             total = total + landed[step - 1, place, :].astype(jnp.float32)
         landed[0, place, :] = total.astype(jnp.bfloat16)
-        store_copy(chunk).start()
+        store_copy(chunk, size, shift).start()
         return carry
 
-    lax.fori_loop(0, CHUNKS, finish, 0)
+    for low, high, size, shift in loops:
+        lax.fori_loop(low, high, functools.partial(finish, size, shift), 0)
     for source, condition, copy in sends:
 
         @pl.when(condition)
         def _(copy=copy):
             copy.wait_send()
 
-    def drain(chunk, carry):
+    def drain(size, shift, chunk, carry):
         for step in range(1, tp_size):
-            term_copy(chunk, step).wait_send()
-        store_copy(chunk).wait()
+            term_copy(chunk, step, size, shift).wait_send()
+        store_copy(chunk, size, shift).wait()
         return carry
 
-    lax.fori_loop(0, CHUNKS, drain, 0)
+    for low, high, size, shift in loops:
+        lax.fori_loop(low, high, functools.partial(drain, size, shift), 0)
 
 
 def on_device(
@@ -402,6 +415,7 @@
             pltpu.VMEM((length, query_rank), low),
             pltpu.VMEM((length, LANES), jnp.float32),
             pltpu.VMEM((length, LANES), jnp.float32),
+            pltpu.VMEM((length, LANES), jnp.int32),
             pltpu.VMEM((length // CHUNKS, window), jnp.float32),
             pltpu.VMEM((length // CHUNKS, heads * LANES), low),
             pltpu.VMEM((length, model), low),
@@ -409,9 +423,9 @@
             pltpu.SemaphoreType.DMA((5,)),
             pltpu.SemaphoreType.DMA((SPAN + 1,)),
             pltpu.SemaphoreType.DMA((14,)),
-            pltpu.SemaphoreType.DMA((max(tp_size - 1, 1), CHUNKS)),
-            pltpu.SemaphoreType.DMA((max(tp_size - 1, 1), CHUNKS)),
-            pltpu.SemaphoreType.DMA((CHUNKS,)),
+            pltpu.SemaphoreType.DMA((max(tp_size - 1, 1), PIECES)),
+            pltpu.SemaphoreType.DMA((max(tp_size - 1, 1), PIECES)),
+            pltpu.SemaphoreType.DMA((PIECES,)),
         ],
         compiler_params=pltpu.CompilerParams(
             collective_id=0, has_side_effects=True, vmem_limit_bytes=60 * 1024 * 1024
@@ -419,8 +433,8 @@
     )(
         query_latent,
         shared_latent,
-        rotary_key,
-        document_start.reshape(length, 1),
+        rotary_key.T,
+        document_start.reshape(1, length),
         query_gain.reshape(1, query_rank),
         shared_gain.reshape(1, shared_rank),
         frequency,

time: 91 us -> 92.7 us (1.019)
  Pallas kernels: 84.7 us -> 89.4 us
  local copies, waits for them, and re-layouts: 6.08 us -> 3.13 us
    pallas_call x1, Pallas kernels: 84.7 us -> 89.4 us  [on_device(): pl.pallas_call(functools.partial(kernel, sp_size, tp_size), out_shape=jax...]
    unnamed x2 -> x1, local copies, waits for them, and re-layouts: 4.61 us -> 3.13 us
    reshape x1 -> x0, local copies, waits for them, and re-layouts: 1.47 us -> none  [on_device(): document_start.reshape(length, 1)]
where the time goes in v2:
time: 92.7 us; the launch traced here: 92.5 us
  Pallas kernels  89.4 us (96%)
  local copies, waits for them, and re-layouts  3.13 us (3%)
    pallas_call x1, Pallas kernels, on_device(): pl.pallas_call(functools.partial(kernel, sp_size, tp_size), out_shape=jax...  89.4 us
    unnamed x1, local copies, waits for them, and re-layouts  3.13 us

profile of v2, /device:TPU:16, one launch (start us, length us, event | category | flops | bytes accessed | tf_op | source)
XLA Modules:
  0.0 92.5 jit_solution(14416270529032550962)
XLA Ops:
  0.0 89.4 %shard_map.118 = bf16[256,4096]{1,0:T(8,128)(2,1)} custom-call(bf16[256,1024]{1,0:T(8,128)(2,1)} %query_ref.1, bf16[256,512]{1,0:T(8,128)(2,1)} %shared_ref.1, bf16[64,256]{1,0:T(8,128)(2,1)} %bitcast.4, s32[1,256]{1,0:T(1,128)} %bitcast.7, f32[1,1024]{1,0:T(1,128)} %bitcast.5, f32[1,512]{1,0:T(1,128)} %bitcast.6, f32[1,128]{1,0:T(1,128)} %constant.2.clone.frequency_ref, ...), custom_call_target="tpu_custom_call" | custom-call | tf_op jit(solution)/shard_map/pallas_call | solution.py:399
  89.4 3.1 %copy.14 = bf16[256,4096]{1,0:T(8,128)(2,1)} copy(bf16[256,4096]{1,0:T(8,128)(2,1)} %shard_map.118) | data formatting | bytes 4194304

commit v3 on v2

--- a/solution.py
+++ b/solution.py
@@ -13,7 +13,6 @@
 SPAN = 8
 LANES = 128
 CHUNKS = 4
-PIECES = CHUNKS + 1
 
 norm_eps = 1e-06
 rope_theta = 10000.0
@@ -274,7 +273,7 @@
     opening = (me - (SPAN - 1)) * length
 
     half = rows // 2
-    loops = ((0, 2, half, 0), (2, PIECES, rows, rows))
+    loops = ((0, CHUNKS, rows, 0),)
 
     def place_of(piece, size, shift):
         return pl.ds(pl.multiple_of(piece * size - shift, half), size)
@@ -318,7 +317,7 @@
             ).astype(jnp.bfloat16)
             return inner
 
-        lax.fori_loop(0, heads, one_head, 0)
+        lax.fori_loop(0, heads, one_head, 0, unroll=2)
         wide = 4 * LANES
 
         def output_columns(j, inner):
@@ -423,9 +422,9 @@
             pltpu.SemaphoreType.DMA((5,)),
             pltpu.SemaphoreType.DMA((SPAN + 1,)),
             pltpu.SemaphoreType.DMA((14,)),
-            pltpu.SemaphoreType.DMA((max(tp_size - 1, 1), PIECES)),
-            pltpu.SemaphoreType.DMA((max(tp_size - 1, 1), PIECES)),
-            pltpu.SemaphoreType.DMA((PIECES,)),
+            pltpu.SemaphoreType.DMA((max(tp_size - 1, 1), CHUNKS)),
+            pltpu.SemaphoreType.DMA((max(tp_size - 1, 1), CHUNKS)),
+            pltpu.SemaphoreType.DMA((CHUNKS,)),
         ],
         compiler_params=pltpu.CompilerParams(
             collective_id=0, has_side_effects=True, vmem_limit_bytes=60 * 1024 * 1024

time: 92.7 us -> 87.3 us (0.942)
  Pallas kernels: 89.4 us -> 84 us
    pallas_call x1, Pallas kernels: 89.4 us -> 84 us  [on_device(): pl.pallas_call(functools.partial(kernel, sp_size, tp_size), out_shape=jax...]
where the time goes in v3:
time: 87.3 us; the launch traced here: 87.1 us
  Pallas kernels  84 us (96%)
  local copies, waits for them, and re-layouts  3.13 us (4%)
    pallas_call x1, Pallas kernels, on_device(): pl.pallas_call(functools.partial(kernel, sp_size, tp_size), out_shape=jax...  84 us
    unnamed x1, local copies, waits for them, and re-layouts  3.13 us

profile of v3, /device:TPU:16, one launch (start us, length us, event | category | flops | bytes accessed | tf_op | source)
XLA Modules:
  0.0 87.1 jit_solution(8631885333677197634)
XLA Ops:
  0.0 84.0 %shard_map.118 = bf16[256,4096]{1,0:T(8,128)(2,1)} custom-call(bf16[256,1024]{1,0:T(8,128)(2,1)} %query_ref.1, bf16[256,512]{1,0:T(8,128)(2,1)} %shared_ref.1, bf16[64,256]{1,0:T(8,128)(2,1)} %bitcast.4, s32[1,256]{1,0:T(1,128)} %bitcast.7, f32[1,1024]{1,0:T(1,128)} %bitcast.5, f32[1,512]{1,0:T(1,128)} %bitcast.6, f32[1,128]{1,0:T(1,128)} %constant.2.clone.frequency_ref, ...), custom_call_target="tpu_custom_call" | custom-call | tf_op jit(solution)/shard_map/pallas_call | solution.py:398
  84.0 3.1 %copy.14 = bf16[256,4096]{1,0:T(8,128)(2,1)} copy(bf16[256,4096]{1,0:T(8,128)(2,1)} %shard_map.118) | data formatting | bytes 4194304
